TPU v7x, 32 devices: a whole 2x2x4 slice. The times are simulated.
32 devices in a mesh: grp: 2 (over x), tp: 4 (over z), dp: 4 (over y, core).
Axes of the slice: x: 2, y: 2, z: 4, core: 2. Of those that a mesh axis runs over, the one named last changes fastest.
Arguments:
- stream: bfloat16 [32, 4096], P('grp', 'dp'), parts along dimension 0, may hold values from -11 to 11
- states: float32 [2, 32, 32, 64, 64], P(None, ('grp', 'dp'), 'tp'), parts along dimension 1, may hold values from -6 to 6
- norm_gain: bfloat16 [2, 4096], P(None, 'dp'), may hold values from 0.099609375 to 1.8984375
- recept_weight: bfloat16 [2, 4096, 2048], P(None, 'dp', 'tp'), may hold values from -0.09375 to 0.09375
- key_weight: bfloat16 [2, 4096, 2048], P(None, 'dp', 'tp'), may hold values from -0.09375 to 0.09375
- value_weight: bfloat16 [2, 4096, 2048], P(None, 'dp', 'tp'), may hold values from -0.09375 to 0.09375
- decay_weight: bfloat16 [2, 4096, 2048], P(None, 'dp', 'tp'), may hold values from -0.09375 to 0.09375
- rate_weight: bfloat16 [2, 4096, 2048], P(None, 'dp', 'tp'), may hold values from -0.09375 to 0.09375
- gate_weight: bfloat16 [2, 4096, 2048], P(None, 'dp', 'tp'), may hold values from -0.09375 to 0.09375
- out_weight: bfloat16 [2, 2048, 4096], P(None, 'tp', 'dp'), may hold values from -0.125 to 0.125
- decay_bias: float32 [2, 2048], P(None, 'tp'), may hold values from -2 to 2
- head_gain: bfloat16 [2, 2048], P(None, 'tp'), may hold values from 0.099609375 to 1.8984375
Outputs:
- new_stream: bfloat16 [32, 4096], P('grp', 'dp'), parts along dimension 0
- new_states: float32 [2, 32, 32, 64, 64], P(None, ('grp', 'dp'), 'tp'), parts along dimension 1
There are 2 independent parts, one for each index of `grp`. A program takes and returns all parts, laid end to end along the dimension named above; an argument that names none is the same for every part. Nothing has to cross between parts.
All inputs are finite; a program needn't handle non-finite values.
Results may differ from a plain program's by a relative error of at most 0.0068.
Values may be sent and summed in bfloat16 or wider, within the bound.
A program may use at most 64 MiB of HBM per device.

v0:
```python
import jax
import jax.numpy as jnp
from jax import lax
from jax.sharding import PartitionSpec as P

D = 4096
HEAD = 64


def run_block(stream, state_blk, gain, weights, out_weight, bias, hgain):
    current = stream.astype(jnp.float32)
    squares = jnp.sum(current * current, axis=1)
    normed = (current * gain.astype(jnp.float32)).astype(jnp.bfloat16)
    width = weights[0].shape[1]
    local_rows = state_blk.shape[0]
    all_totals = lax.psum(squares, "dp")
    offset = lax.axis_index("dp") * local_rows
    totals = lax.dynamic_slice_in_dim(all_totals, offset, local_rows, 0)
    summed = lax.psum_scatter(
        jnp.concatenate(
            [jnp.dot(normed, weight, preferred_element_type=jnp.float32) for weight in weights],
            axis=1,
        ),
        "dp",
        scatter_dimension=0,
        tiled=True,
    )
    inv_rms = lax.rsqrt(totals / D + 1e-06)[:, None]
    projected = (summed * inv_rms).reshape(local_rows, 6, -1, HEAD)
    recept = projected[:, 0]
    key_vec = projected[:, 1]
    value_vec = projected[:, 2]
    decay_pre = projected[:, 3]
    rate_pre = projected[:, 4]
    gate_pre = projected[:, 5]
    unit_key = key_vec * lax.rsqrt(jnp.sum(key_vec * key_vec, axis=2, keepdims=True) + 1e-06)
    rate_vec = jax.nn.sigmoid(rate_pre)
    decay = jnp.exp(-0.606531 * jax.nn.sigmoid(bias.reshape(1, -1, HEAD) + decay_pre))
    removed = jnp.einsum("bhij,bhj->bhi", state_blk, unit_key, precision=lax.Precision.HIGHEST)
    new_state = (
        state_blk * decay[:, :, None, :]
        - removed[..., None] * (unit_key * rate_vec)[:, :, None, :]
        + value_vec[..., None] * key_vec[:, :, None, :]
    )
    read = jnp.einsum("bhij,bhj->bhi", new_state, recept, precision=lax.Precision.HIGHEST)
    center = read - jnp.mean(read, axis=2, keepdims=True)
    normal_read = center * lax.rsqrt(jnp.mean(center * center, axis=2, keepdims=True) + 1e-05)
    gated = normal_read * hgain.astype(jnp.float32).reshape(1, -1, HEAD) * jax.nn.sigmoid(gate_pre)
    mixed = gated.reshape(local_rows, width).astype(jnp.bfloat16)
    branch_part = jnp.dot(
        lax.all_gather(mixed, "dp", axis=0, tiled=True),
        out_weight,
        preferred_element_type=jnp.float32,
    )
    branch = lax.psum(branch_part, "tp")
    return ((current + branch).astype(jnp.bfloat16), new_state)


def per_device(
    stream,
    states,
    norm_gain,
    recept_weight,
    key_weight,
    value_weight,
    decay_weight,
    rate_weight,
    gate_weight,
    out_weight,
    decay_bias,
    head_gain,
):
    current = stream
    fresh_list = []
    for layer in range(2):
        weights = (
            recept_weight[layer],
            key_weight[layer],
            value_weight[layer],
            decay_weight[layer],
            rate_weight[layer],
            gate_weight[layer],
        )
        current, fresh = run_block(
            current,
            states[layer],
            norm_gain[layer],
            weights,
            out_weight[layer],
            decay_bias[layer],
            head_gain[layer],
        )
        fresh_list.append(fresh)
    return (current, jnp.stack(fresh_list))


def solution(mesh):
    in_specs = (
        P("grp", "dp"),
        P(None, ("grp", "dp"), "tp", None, None),
        P(None, "dp"),
        P(None, "dp", "tp"),
        P(None, "dp", "tp"),
        P(None, "dp", "tp"),
        P(None, "dp", "tp"),
        P(None, "dp", "tp"),
        P(None, "dp", "tp"),
        P(None, "tp", "dp"),
        P(None, "tp"),
        P(None, "tp"),
    )
    out_specs = (P("grp", "dp"), P(None, ("grp", "dp"), "tp", None, None))
    return jax.shard_map(
        per_device, mesh=mesh, in_specs=in_specs, out_specs=out_specs, check_vma=False
    )
```

profile of v0, /device:TPU:0, one launch (start us, length us, event | category | flops | bytes accessed | tf_op | source)
XLA Modules:
  0.0 201.3 jit_solution(15151777179491624203)
XLA Ops:
  7.2 0.0 all-reduce.11.cloned.1.call-start
  7.2 0.9 slice_convert_fusion
  8.1 1.6 convolution_dynamic-update-slice_fusion.11
  9.7 1.5 convolution_dynamic-update-slice_fusion.10
  11.3 0.2 convolution_dynamic-update-slice_fusion.9
  11.5 1.6 convolution_dynamic-update-slice_fusion.8
  13.1 0.3 convolution_dynamic-update-slice_fusion.7
  13.4 1.5 convolution_dynamic-update-slice_fusion.6
  14.9 0.7 copy-done.6
  15.6 0.0 all-reduce.11.cloned.1.call-update
  15.6 0.0 all-reduce.7.cloned.1.call-start
  15.6 0.1 fusion.61
  15.8 8.4 %psum.28 = f32[16]{0:T(128)S(1)} all-reduce(f32[16]{0:T(128)S(1)} %fusion.61), channel_id=1, replica_groups=mesh['grp'=2,'tp'=4,'dp'=4] {'dp'}, use_global_device_ids=true, to_apply=%region_2.0 | all-reduce | flops 16 | bytes 128 | tf_op jit(solution)/shard_map/psum | solution.py:16
  24.2 0.1 reshape.165
  24.3 0.1 add.138
  24.4 0.6 dynamic-slice
  25.6 0.1 add_rsqrt_fusion.5
  25.7 24.8 %all-reduce.11.cloned.1.call-done = f32[16,3072]{1,0:T(8,128)} async-done(((f32[16,3072]{1,0:T(8,128)}), f32[16,3072]{1,0:T(8,128)}) %all-reduce.11.cloned.1.call-update) | async-done | bytes 196624
  50.5 1.0 dynamic-slice_multiply_fusion.1
  51.4 0.1 reshape.162
  51.5 0.1 fusion.99
  51.6 0.1 fusion.92
  51.7 1.7 fusion.22
  53.5 2.1 %fusion.26 = f32[4,8,1,64]{3,2,1,0:T(1,128)S(1)} fusion(f32[4,8,64,1]{2,3,1,0:T(1,128)S(1)} %bitcast.192, f32[2,4,8,64,64]{4,3,2,1,0:T(8,128)S(1)} %copy-done, f32[4,8,64]{2,1,0:T(8,128)S(1)} %get-tuple-element.23, f32[4,8,64]{2,1,0:T(8,128)S(1)} %get-tuple-element.21, f32[4,8,64]{2,1,0:T(8,128)S(1)} %get-tuple-element.10, f32[4,8,64]{2,1,0:T(8,128)S(1)} %bitcast.185, ...), kind=kOutput, calls=%fused_computation.40 | convolution fusion | flops 2228224 | bytes 1155072 | tf_op jit(solution)/shard_map/bhij,bhj->bhi/dot_general | solution.py:45
  55.5 0.1 reduce_sum.74
  55.6 0.2 multiply_reduce_fusion.2
  55.8 0.1 fusion.100
  55.9 0.1 reshape.168
  56.0 5.2 %all-gather = bf16[4,4,512]{2,1,0:T(4,128)(2,1)S(1)} all-gather(bf16[1,4,512]{2,1,0:T(4,128)(2,1)S(1)} %reshape.168), channel_id=1, replica_groups=mesh['grp'=2,'tp'=4,'dp'=4] {'dp'}, dimensions={0}, use_global_device_ids=true | all-gather | bytes 20480 | tf_op jit(solution)/shard_map/all_gather | solution.py:51
  61.2 2.1 %fusion.14 = f32[16,1024]{1,0:T(8,128)} fusion(bf16[16,512]{1,0:T(8,128)(2,1)S(1)} %reshape.169, bf16[2,512,1024]{2,1,0:T(8,128)(2,1)} %param.21), kind=kOutput, calls=%fused_computation.27 | convolution fusion | flops 16777216 | bytes 1130496 | tf_op jit(solution)/shard_map/dot_general | solution.py:50
  63.3 0.0 all-reduce.7.cloned.1.call-update
  63.3 0.0 all-reduce.13.cloned.1.call-start
  63.4 0.1 reshape.167
  63.5 0.1 add.150
  63.5 34.3 %all-reduce.7.cloned.1.call-done = f32[16,1024]{1,0:T(8,128)} async-done(((f32[16,1024]{1,0:T(8,128)}), f32[16,1024]{1,0:T(8,128)}) %all-reduce.7.cloned.1.call-update) | async-done | bytes 65552 | tf_op jit(solution)/shard_map/psum | solution.py:55
  97.8 1.0 fusion.64
  98.8 5.7 %psum.30 = f32[16]{0:T(128)S(1)} all-reduce(f32[16]{0:T(128)S(1)} %get-tuple-element.8), channel_id=1, replica_groups=mesh['grp'=2,'tp'=4,'dp'=4] {'dp'}, use_global_device_ids=true, to_apply=%region_9.0 | all-reduce | flops 16 | bytes 128 | tf_op jit(solution)/shard_map/psum | solution.py:16
  104.4 1.6 convolution_dynamic-update-slice_fusion.5
  106.1 1.5 convolution_dynamic-update-slice_fusion.4
  107.5 0.3 convolution_dynamic-update-slice_fusion.3
  107.8 1.5 convolution_dynamic-update-slice_fusion.2
  109.3 0.3 convolution_dynamic-update-slice_fusion.1
  109.5 1.5 convolution_dynamic-update-slice_fusion
  111.0 0.7 copy-done.7
  111.7 0.0 all-reduce.13.cloned.1.call-update
  111.7 0.0 all-reduce.9.cloned.1.call-start
  111.8 0.1 add_rsqrt_fusion.4
  111.8 32.0 %all-reduce.13.cloned.1.call-done = f32[16,3072]{1,0:T(8,128)} async-done(((f32[16,3072]{1,0:T(8,128)}), f32[16,3072]{1,0:T(8,128)}) %all-reduce.13.cloned.1.call-update) | async-done | bytes 196624
  143.8 1.0 dynamic-slice_multiply_fusion
  144.8 0.1 reshape.163
  144.9 0.1 fusion.82
  145.0 0.1 fusion.75
  145.1 1.7 fusion.8
  146.8 2.2 %multiply_add_fusion.1 = (f32[1,4,8,64,64]{4,3,2,1,0:T(8,128)S(1)}, f32[1,4,8,64,64]{4,3,2,1,0:T(8,128)}) fusion(f32[2,4,8,64,64]{4,3,2,1,0:T(8,128)S(1)} %copy-done, f32[4,8,64]{2,1,0:T(8,128)S(1)} %get-tuple-element.23, f32[4,8,64]{2,1,0:T(8,128)S(1)} %get-tuple-element.21, f32[4,8,64]{2,1,0:T(8,128)S(1)} %get-tuple-element.10, ...), kind=kLoop, calls=%fused_computation.42 | loop fusion | flops 1310720 | bytes 2179072 | tf_op jit(solution)/shard_map/add | solution.py:41
  149.0 2.1 %fusion.12 = f32[4,8,1,64]{3,2,1,0:T(1,128)S(1)} fusion(f32[4,8,64,1]{2,3,1,0:T(1,128)S(1)} %bitcast.191, f32[2,4,8,64,64]{4,3,2,1,0:T(8,128)S(1)} %copy-done, f32[4,8,64]{2,1,0:T(8,128)S(1)} %get-tuple-element.18, f32[4,8,64]{2,1,0:T(8,128)S(1)} %get-tuple-element.16, f32[4,8,64]{2,1,0:T(8,128)S(1)} %get-tuple-element.6, f32[4,8,64]{2,1,0:T(8,128)S(1)} %bitcast.188, ...), kind=kOutput, calls=%fused_computation.26 | convolution fusion | flops 2228224 | bytes 1155072 | tf_op jit(solution)/shard_map/bhij,bhj->bhi/dot_general | solution.py:45
  151.1 0.1 reduce_sum.78
  151.2 0.2 multiply_reduce_fusion
  151.4 0.1 fusion.101
  151.4 0.1 reshape.170
  151.5 5.2 %all-gather.1 = bf16[4,4,512]{2,1,0:T(4,128)(2,1)S(1)} all-gather(bf16[1,4,512]{2,1,0:T(4,128)(2,1)S(1)} %reshape.170), channel_id=1, replica_groups=mesh['grp'=2,'tp'=4,'dp'=4] {'dp'}, dimensions={0}, use_global_device_ids=true | all-gather | bytes 20480 | tf_op jit(solution)/shard_map/all_gather | solution.py:51
  156.8 2.1 %fusion = f32[16,1024]{1,0:T(8,128)} fusion(bf16[16,512]{1,0:T(8,128)(2,1)S(1)} %reshape.171, bf16[2,512,1024]{2,1,0:T(8,128)(2,1)} %param.21), kind=kOutput, calls=%fused_computation.13 | convolution fusion | flops 16777216 | bytes 1130496 | tf_op jit(solution)/shard_map/dot_general | solution.py:50
  158.9 2.8 %pad_maximum_fusion = f32[2,4,8,64,64]{4,3,2,1,0:T(8,128)} fusion(f32[1,4,8,64,64]{4,3,2,1,0:T(8,128)} %get-tuple-element.13, f32[1,4,8,64,64]{4,3,2,1,0:T(8,128)S(1)} %get-tuple-element.12), kind=kLoop, calls=%fused_computation | loop fusion | flops 262144 | bytes 2097152 | tf_op jit(solution)/shard_map/stack | solution.py:94
  161.6 31.7 %all-reduce.9.cloned.1.call-done = f32[16,1024]{1,0:T(8,128)} async-done(((f32[16,1024]{1,0:T(8,128)}), f32[16,1024]{1,0:T(8,128)}) %all-reduce.9.cloned.1.call-update) | async-done | bytes 65552 | tf_op jit(solution)/shard_map/psum | solution.py:55
  193.3 1.5 fusion.65
  (32 shorter events, 0.2 us)
Async XLA Ops:
  7.2 4.1 %copy-start.1 = (bf16[16,1024]{1,0:T(8,128)(2,1)S(1)}, bf16[16,1024]{1,0:T(8,128)(2,1)}, u32[]{:S(2)}) copy-start(bf16[16,1024]{1,0:T(8,128)(2,1)} %param.12) | copy-start | bytes 98308
  7.2 4.1 %copy-start.2 = (bf16[2,1024,512]{2,1,0:T(8,128)(2,1)S(1)}, bf16[2,1024,512]{2,1,0:T(8,128)(2,1)}, u32[]{:S(2)}) copy-start(bf16[2,1024,512]{2,1,0:T(8,128)(2,1)} %param.17) | copy-start | bytes 6291460
  7.2 43.3 %all-reduce.11.cloned.1.call-start = ((), (), s32[]{:S(2)}) async-start(), calls=%async_computation.2 | async-start | bytes 393216
  8.1 5.0 %copy-start.4 = (bf16[2,1024,512]{2,1,0:T(8,128)(2,1)S(1)}, bf16[2,1024,512]{2,1,0:T(8,128)(2,1)}, u32[]{:S(2)}) copy-start(bf16[2,1024,512]{2,1,0:T(8,128)(2,1)} %param.19) | copy-start | bytes 6291460
  11.2 12.9 %copy-start.8 = (bf16[2,512]{1,0:T(2,128)(2,1)S(1)}, bf16[2,512]{1,0:T(2,128)(2,1)}, u32[]{:S(2)}) copy-start(bf16[2,512]{1,0:T(2,128)(2,1)} %param.23) | copy-start | bytes 6148
  11.2 12.9 %copy-start.9 = (f32[2,512]{1,0:T(2,128)S(1)}, f32[2,512]{1,0:T(2,128)}, u32[]{:S(2)}) copy-start(f32[2,512]{1,0:T(2,128)} %param.22) | copy-start | bytes 12292
  11.5 12.9 %copy-start.10 = (u32[32]{0:T(128)S(1)}, u32[32]{0:T(128)}, u32[]{:S(2)}) copy-start(u32[32]{0:T(128)} %constant.34) | copy-start | bytes 388
  11.5 40.2 %copy-start = (f32[2,4,8,64,64]{4,3,2,1,0:T(8,128)S(1)}, f32[2,4,8,64,64]{4,3,2,1,0:T(8,128)}, u32[]{:S(2)}) copy-start(f32[2,4,8,64,64]{4,3,2,1,0:T(8,128)} %param.13) | copy-start | bytes 3145732
  14.9 0.7 copy-start.6
  15.6 82.2 %all-reduce.7.cloned.1.call-start = ((), (), s32[]{:S(2)}) async-start(), calls=%async_computation | async-start | bytes 131072 | tf_op jit(solution)/shard_map/psum | solution.py:55
  63.3 80.5 %all-reduce.13.cloned.1.call-start = ((), (), s32[]{:S(2)}) async-start(), calls=%async_computation.3 | async-start | bytes 393216
  104.4 3.1 %copy-start.3 = (bf16[2,1024,512]{2,1,0:T(8,128)(2,1)S(1)}, bf16[2,1024,512]{2,1,0:T(8,128)(2,1)}, u32[]{:S(2)}) copy-start(bf16[2,1024,512]{2,1,0:T(8,128)(2,1)} %param.17) | copy-start | bytes 6291460
  104.4 4.8 %copy-start.5 = (bf16[2,1024,512]{2,1,0:T(8,128)(2,1)S(1)}, bf16[2,1024,512]{2,1,0:T(8,128)(2,1)}, u32[]{:S(2)}) copy-start(bf16[2,1024,512]{2,1,0:T(8,128)(2,1)} %param.19) | copy-start | bytes 6291460
  111.0 0.7 copy-start.7
  111.7 81.6 %all-reduce.9.cloned.1.call-start = ((), (), s32[]{:S(2)}) async-start(), calls=%async_computation.1 | async-start | bytes 131072 | tf_op jit(solution)/shard_map/psum | solution.py:55
Sparse Core Ops, SparseCore 0:
  15.7 34.7 all-reduce.10
  63.5 34.3 all-reduce.6
  111.8 31.9 all-reduce.12
  159.0 34.2 all-reduce.8
where the time goes:
time: 202 us; the launch traced here: 201 us
  waiting for transfers between devices  123 us (61%)
  matrix products  25.1 us (12%)
  blocking collectives  24.5 us (12%)
  between operations  14.5 us (7%)
  other arithmetic  11.5 us (6%)
  local copies, waits for them, and re-layouts  2.74 us (1%)
    psum x2, waiting for transfers between devices, run_block(): branch = lax.psum(branch_part, 'tp')  66 us
    unnamed x6, waiting for transfers between devices  56.8 us
    psum x2, blocking collectives, run_block(): all_totals = lax.psum(squares, 'dp')  14.1 us
    dot_general x12, matrix products, run_block(): jnp.dot(normed, weight, preferred_element_type=jnp.float32)  13.3 us
    all_gather x2, blocking collectives, run_block(): lax.all_gather(mixed, 'dp', axis=0, tiled=True)  10.4 us
    dot_general x2, matrix products, run_block(): jnp.dot(lax.all_gather(mixed, 'dp', axis=0, tiled=True), out_weight, pref...  4.2 us
    dot_general x2, matrix products, run_block(): jnp.einsum('bhij,bhj->bhi', new_state, recept, precision=lax.Precision.HI...  4.16 us
  transfers between devices with their start and end apart: 4, of which 4 were waited for; matrix products, arithmetic and copies ran while one was open for 2% of the time, Pallas kernels for 0%

commit v1 on v0

--- a/solution.py
+++ b/solution.py
@@ -52,7 +52,9 @@
         out_weight,
         preferred_element_type=jnp.float32,
     )
-    branch = lax.psum(branch_part, "tp")
+    branch = branch_part
+    for hop in (1, 2):
+        branch = branch + lax.ppermute(branch, "tp", [(dev, dev ^ hop) for dev in range(4)])
     return ((current + branch).astype(jnp.bfloat16), new_state)
 
 

time: 202 us -> 148 us (0.73)
  waiting for transfers between devices: 123 us -> 65.9 us
  starting transfers between devices: 0.16 us -> 8 us
  other arithmetic: 11.5 us -> 7.82 us
    psum x2 -> x0, waiting for transfers between devices: 66 us -> none  [run_block(): branch = lax.psum(branch_part, 'tp')]
    ppermute x0 -> x4, waiting for transfers between devices: none -> 8.45 us  [run_block(): lax.ppermute(branch, 'tp', [(dev, dev ^ hop) for dev in range(4)])]
    ppermute x0 -> x4, starting transfers between devices: none -> 7.92 us  [run_block(): lax.ppermute(branch, 'tp', [(dev, dev ^ hop) for dev in range(4)])]
    unnamed x6 -> x4, waiting for transfers between devices: 56.8 us -> 57.5 us
  transfers between devices with their start and end apart: 4 -> 6, of which waited for: 4 -> 6; matrix products, arithmetic and copies ran while one was open for 2% -> 3% of each run, Pallas kernels for 0% -> 0%
where the time goes in v1:
time: 148 us
  waiting for transfers between devices  65.9 us (45%)
  blocking collectives  24.7 us (17%)
  matrix products  23.9 us (16%)
  between operations  14.8 us (10%)
  starting transfers between devices  8 us (5%)
  other arithmetic  7.82 us (5%)
  local copies, waits for them, and re-layouts  2.74 us (2%)
    unnamed x4, waiting for transfers between devices  57.5 us
    psum x2, blocking collectives, run_block(): all_totals = lax.psum(squares, 'dp')  14.3 us
    dot_general x12, matrix products, run_block(): jnp.dot(normed, weight, preferred_element_type=jnp.float32)  13.3 us
    all_gather x2, blocking collectives, run_block(): lax.all_gather(mixed, 'dp', axis=0, tiled=True)  10.4 us
    ppermute x4, waiting for transfers between devices, run_block(): lax.ppermute(branch, 'tp', [(dev, dev ^ hop) for dev in range(4)])  8.45 us
    ppermute x4, starting transfers between devices, run_block(): lax.ppermute(branch, 'tp', [(dev, dev ^ hop) for dev in range(4)])  7.92 us
    dot_general x2, matrix products, run_block(): jnp.einsum('bhij,bhj->bhi', new_state, recept, precision=lax.Precision.HI...  4.17 us
    dot_general x2, matrix products, run_block(): jnp.einsum('bhij,bhj->bhi', state_blk, unit_key, precision=lax.Precision....  3.49 us
  transfers between devices with their start and end apart: 6, of which 6 were waited for; matrix products, arithmetic and copies ran while one was open for 3% of the time, Pallas kernels for 0%

profile of v1, /device:TPU:0, one launch (start us, length us, event | category | flops | bytes accessed | tf_op | source)
XLA Modules:
  0.0 147.8 jit_solution(5149260639286493216)
XLA Ops:
  7.2 0.9 slice_convert_fusion
  8.1 1.6 %convolution_dynamic-update-slice_fusion.11 = f32[16,3072]{1,0:T(8,128)S(1)} fusion(bf16[2,1024,512]{2,1,0:T(8,128)(2,1)} %param.15, bf16[16,1024]{1,0:T(8,128)(2,1)} %param.12, f32[1024]{0:T(1024)S(1)} %bitcast.173), kind=kOutput, calls=%fused_computation.12 | convolution fusion | flops 16826368 | bytes 1118208 | tf_op jit(solution)/shard_map/dot_general | solution.py:21
  9.7 1.5 %convolution_dynamic-update-slice_fusion.10 = f32[16,3072]{1,0:T(8,128)S(1)} fusion(f32[16,3072]{1,0:T(8,128)S(1)} %convolution_dynamic-update-slice_fusion.11, bf16[2,1024,512]{2,1,0:T(8,128)(2,1)} %param.16, bf16[16,1024]{1,0:T(8,128)(2,1)} %param.12, f32[1024]{0:T(1024)S(1)} %bitcast.174), kind=kOutput, calls=%fused_computation.11 | convolution fusion | flops 16826368 | bytes 1118208 | tf_op jit(solution)/shard_map/dot_general | solution.py:21
  11.3 0.2 convolution_dynamic-update-slice_fusion.9
  11.5 1.6 %convolution_dynamic-update-slice_fusion.8 = f32[16,3072]{1,0:T(8,128)S(1)} fusion(f32[16,3072]{1,0:T(8,128)S(1)} %convolution_dynamic-update-slice_fusion.9, bf16[2,1024,512]{2,1,0:T(8,128)(2,1)} %param.18, bf16[16,1024]{1,0:T(8,128)(2,1)S(1)} %copy-done.1, f32[1024]{0:T(1024)S(1)} %bitcast.176), kind=kOutput, calls=%fused_computation.9 | convolution fusion | flops 16826368 | bytes 1118208 | tf_op jit(solution)/shard_map/dot_general | solution.py:21
  13.1 0.3 convolution_dynamic-update-slice_fusion.7
  13.4 1.5 convolution_dynamic-update-slice_fusion.6
  14.9 0.7 copy-done.6
  15.6 0.0 all-reduce.7.cloned.1.call-start
  15.6 0.1 fusion.61
  15.8 8.4 %psum.14 = f32[16]{0:T(128)S(1)} all-reduce(f32[16]{0:T(128)S(1)} %fusion.61), channel_id=1, replica_groups=mesh['grp'=2,'tp'=4,'dp'=4] {'dp'}, use_global_device_ids=true, to_apply=%region_2.0 | all-reduce | flops 16 | bytes 128 | tf_op jit(solution)/shard_map/psum | solution.py:16
  24.2 0.1 reshape.165
  24.3 0.1 add.146
  24.4 0.6 dynamic-slice
  25.6 0.1 add_rsqrt_fusion.5
  25.7 24.8 %all-reduce.5.cloned.1.call-done = f32[16,3072]{1,0:T(8,128)} async-done(((f32[16,3072]{1,0:T(8,128)}), f32[16,3072]{1,0:T(8,128)}) %all-reduce.5.cloned.1.call-update) | async-done | bytes 196624
  50.5 1.0 dynamic-slice_multiply_fusion.1
  51.4 0.1 reshape.162
  51.5 0.1 fusion.99
  51.6 0.1 fusion.92
  51.7 1.7 %fusion.22 = f32[4,8,1,64]{3,2,1,0:T(1,128)S(1)} fusion(f32[4,8,64,1]{2,3,1,0:T(1,128)S(1)} %bitcast.189, f32[2,4,8,64,64]{4,3,2,1,0:T(8,128)S(1)} %copy-done), kind=kOutput, calls=%fused_computation.35 | convolution fusion | flops 1572864 | bytes 1073152 | tf_op jit(solution)/shard_map/bhij,bhj->bhi/dot_general | solution.py:39
  53.5 2.1 %fusion.26 = f32[4,8,1,64]{3,2,1,0:T(1,128)S(1)} fusion(f32[4,8,64,1]{2,3,1,0:T(1,128)S(1)} %bitcast.191, f32[2,4,8,64,64]{4,3,2,1,0:T(8,128)S(1)} %copy-done, f32[4,8,64]{2,1,0:T(8,128)S(1)} %get-tuple-element.23, f32[4,8,64]{2,1,0:T(8,128)S(1)} %get-tuple-element.21, f32[4,8,64]{2,1,0:T(8,128)S(1)} %get-tuple-element.10, f32[4,8,64]{2,1,0:T(8,128)S(1)} %bitcast.185, ...), kind=kOutput, calls=%fused_computation.40 | convolution fusion | flops 2228224 | bytes 1155072 | tf_op jit(solution)/shard_map/bhij,bhj->bhi/dot_general | solution.py:45
  55.5 0.1 reduce_sum.74
  55.6 0.2 multiply_reduce_fusion.2
  55.8 0.1 fusion.100
  55.9 0.1 reshape.168
  56.0 5.2 %all-gather = bf16[4,4,512]{2,1,0:T(4,128)(2,1)S(1)} all-gather(bf16[1,4,512]{2,1,0:T(4,128)(2,1)S(1)} %reshape.168), channel_id=1, replica_groups=mesh['grp'=2,'tp'=4,'dp'=4] {'dp'}, dimensions={0}, use_global_device_ids=true | all-gather | bytes 20480 | tf_op jit(solution)/shard_map/all_gather | solution.py:51
  61.2 1.5 fusion.14
  62.7 1.5 %collective-permute-start = (f32[16,1024]{1,0:T(8,128)S(1)}, f32[16,1024]{1,0:T(8,128)S(1)}, u32[]{:S(2)}, u32[]{:S(2)}) collective-permute-start(f32[16,1024]{1,0:T(8,128)S(1)} %fusion.14), channel_id=1, source_target_pairs={{0,4},{4,0},{8,12},{12,8},{1,5},{5,1},{9,13},{13,9},{2,6},{6,2},{1... | collective-permute-start | bytes 196616 | tf_op jit(solution)/shard_map/ppermute | solution.py:57
  64.2 2.9 %collective-permute-done = f32[16,1024]{1,0:T(8,128)S(1)} collective-permute-done((f32[16,1024]{1,0:T(8,128)S(1)}, f32[16,1024]{1,0:T(8,128)S(1)}, u32[]{:S(2)}, u32[]{:S(2)}) %collective-permute-start) | collective-permute-done | bytes 65568 | tf_op jit(solution)/shard_map/ppermute | solution.py:57
  67.0 2.5 %collective-permute-start.1 = (f32[16,1024]{1,0:T(8,128)S(1)}, f32[16,1024]{1,0:T(8,128)S(1)}, u32[]{:S(2)}, u32[]{:S(2)}) collective-permute-start(f32[16,1024]{1,0:T(8,128)S(1)} %add.157), channel_id=1, source_target_pairs={{0,8},{4,12},{8,0},{12,4},{1,9},{5,13},{9,1},{13,5},{2,10},{6,14},... | collective-permute-start | bytes 196616 | tf_op jit(solution)/shard_map/ppermute | solution.py:57
  69.5 0.1 reshape.167
  69.6 0.1 add.160
  69.7 2.7 %collective-permute-done.1 = f32[16,1024]{1,0:T(8,128)S(1)} collective-permute-done((f32[16,1024]{1,0:T(8,128)S(1)}, f32[16,1024]{1,0:T(8,128)S(1)}, u32[]{:S(2)}, u32[]{:S(2)}) %collective-permute-start.1) | collective-permute-done | bytes 65568 | tf_op jit(solution)/shard_map/ppermute | solution.py:57
  72.4 0.1 fusion.64
  72.5 5.9 %psum.15 = f32[16]{0:T(128)S(1)} all-reduce(f32[16]{0:T(128)S(1)} %get-tuple-element.8), channel_id=1, replica_groups=mesh['grp'=2,'tp'=4,'dp'=4] {'dp'}, use_global_device_ids=true, to_apply=%region_8.0 | all-reduce | flops 16 | bytes 128 | tf_op jit(solution)/shard_map/psum | solution.py:16
  78.4 1.6 %convolution_dynamic-update-slice_fusion.5 = f32[16,3072]{1,0:T(8,128)S(1)} fusion(bf16[2,1024,512]{2,1,0:T(8,128)(2,1)} %param.15, bf16[16,1024]{1,0:T(8,128)(2,1)S(1)} %get-tuple-element.9, f32[1024]{0:T(1024)S(1)} %bitcast.167), kind=kOutput, calls=%fused_computation.6 | convolution fusion | flops 16826368 | bytes 1118208 | tf_op jit(solution)/shard_map/dot_general | solution.py:21
  80.0 1.5 convolution_dynamic-update-slice_fusion.4
  81.5 0.3 convolution_dynamic-update-slice_fusion.3
  81.8 1.5 convolution_dynamic-update-slice_fusion.2
  83.2 0.3 convolution_dynamic-update-slice_fusion.1
  83.5 1.5 convolution_dynamic-update-slice_fusion
  85.0 0.7 copy-done.7
  85.7 0.1 add_rsqrt_fusion.4
  85.8 32.6 %all-reduce.7.cloned.1.call-done = f32[16,3072]{1,0:T(8,128)} async-done(((f32[16,3072]{1,0:T(8,128)}), f32[16,3072]{1,0:T(8,128)}) %all-reduce.7.cloned.1.call-update) | async-done | bytes 196624
  118.4 1.0 dynamic-slice_multiply_fusion
  119.4 0.1 reshape.163
  119.5 0.1 fusion.82
  119.6 0.1 fusion.75
  119.7 1.7 %fusion.8 = f32[4,8,1,64]{3,2,1,0:T(1,128)S(1)} fusion(f32[4,8,64,1]{2,3,1,0:T(1,128)S(1)} %bitcast.190, f32[2,4,8,64,64]{4,3,2,1,0:T(8,128)S(1)} %copy-done), kind=kOutput, calls=%fused_computation.21 | convolution fusion | flops 1572864 | bytes 1073152 | tf_op jit(solution)/shard_map/bhij,bhj->bhi/dot_general | solution.py:39
  121.4 2.1 %fusion.12 = f32[4,8,1,64]{3,2,1,0:T(1,128)S(1)} fusion(f32[4,8,64,1]{2,3,1,0:T(1,128)S(1)} %bitcast.192, f32[2,4,8,64,64]{4,3,2,1,0:T(8,128)S(1)} %copy-done, f32[4,8,64]{2,1,0:T(8,128)S(1)} %get-tuple-element.18, f32[4,8,64]{2,1,0:T(8,128)S(1)} %get-tuple-element.16, f32[4,8,64]{2,1,0:T(8,128)S(1)} %get-tuple-element.6, f32[4,8,64]{2,1,0:T(8,128)S(1)} %bitcast.187, ...), kind=kOutput, calls=%fused_computation.26 | convolution fusion | flops 2228224 | bytes 1155072 | tf_op jit(solution)/shard_map/bhij,bhj->bhi/dot_general | solution.py:45
  123.5 0.1 reduce_sum.78
  123.6 0.2 multiply_reduce_fusion
  123.8 0.1 fusion.101
  123.8 0.1 reshape.170
  123.9 5.2 %all-gather.1 = bf16[4,4,512]{2,1,0:T(4,128)(2,1)S(1)} all-gather(bf16[1,4,512]{2,1,0:T(4,128)(2,1)S(1)} %reshape.170), channel_id=1, replica_groups=mesh['grp'=2,'tp'=4,'dp'=4] {'dp'}, dimensions={0}, use_global_device_ids=true | all-gather | bytes 20480 | tf_op jit(solution)/shard_map/all_gather | solution.py:51
  129.1 1.5 fusion
  130.6 1.5 %collective-permute-start.2 = (f32[16,1024]{1,0:T(8,128)S(1)}, f32[16,1024]{1,0:T(8,128)S(1)}, u32[]{:S(2)}, u32[]{:S(2)}) collective-permute-start(f32[16,1024]{1,0:T(8,128)S(1)} %fusion), channel_id=1, source_target_pairs={{0,4},{4,0},{8,12},{12,8},{1,5},{5,1},{9,13},{13,9},{2,6},{6,2},{1... | collective-permute-start | bytes 196616 | tf_op jit(solution)/shard_map/ppermute | solution.py:57
  132.1 1.4 multiply_add_fusion.1
  133.5 1.4 collective-permute-done.2
  135.0 2.5 %collective-permute-start.3 = (f32[16,1024]{1,0:T(8,128)S(1)}, f32[16,1024]{1,0:T(8,128)S(1)}, u32[]{:S(2)}, u32[]{:S(2)}) collective-permute-start(f32[16,1024]{1,0:T(8,128)S(1)} %add.170), channel_id=1, source_target_pairs={{0,8},{4,12},{8,0},{12,4},{1,9},{5,13},{9,1},{13,5},{2,10},{6,14},... | collective-permute-start | bytes 196616 | tf_op jit(solution)/shard_map/ppermute | solution.py:57
  137.5 1.5 %pad_maximum_fusion = f32[2,4,8,64,64]{4,3,2,1,0:T(8,128)} fusion(f32[1,4,8,64,64]{4,3,2,1,0:T(8,128)S(1)} %get-tuple-element.13, f32[1,4,8,64,64]{4,3,2,1,0:T(8,128)S(1)} %get-tuple-element.12), kind=kLoop, calls=%fused_computation | loop fusion | flops 262144 | bytes 2097152 | tf_op jit(solution)/shard_map/stack | solution.py:96
  138.9 1.4 collective-permute-done.3
  140.4 0.6 fusion.65
  (36 shorter events, 0.3 us)
Async XLA Ops:
  7.2 4.1 %copy-start.1 = (bf16[16,1024]{1,0:T(8,128)(2,1)S(1)}, bf16[16,1024]{1,0:T(8,128)(2,1)}, u32[]{:S(2)}) copy-start(bf16[16,1024]{1,0:T(8,128)(2,1)} %param.12) | copy-start | bytes 98308
  7.2 4.1 %copy-start.2 = (bf16[2,1024,512]{2,1,0:T(8,128)(2,1)S(1)}, bf16[2,1024,512]{2,1,0:T(8,128)(2,1)}, u32[]{:S(2)}) copy-start(bf16[2,1024,512]{2,1,0:T(8,128)(2,1)} %param.17) | copy-start | bytes 6291460
  7.2 43.3 %all-reduce.5.cloned.1.call-start = ((), (), s32[]{:S(2)}) async-start(), calls=%async_computation | async-start | bytes 393216
  8.1 5.0 %copy-start.4 = (bf16[2,1024,512]{2,1,0:T(8,128)(2,1)S(1)}, bf16[2,1024,512]{2,1,0:T(8,128)(2,1)}, u32[]{:S(2)}) copy-start(bf16[2,1024,512]{2,1,0:T(8,128)(2,1)} %param.19) | copy-start | bytes 6291460
  11.2 12.9 %copy-start.8 = (bf16[2,512]{1,0:T(2,128)(2,1)S(1)}, bf16[2,512]{1,0:T(2,128)(2,1)}, u32[]{:S(2)}) copy-start(bf16[2,512]{1,0:T(2,128)(2,1)} %param.23) | copy-start | bytes 6148
  11.2 12.9 %copy-start.9 = (f32[2,512]{1,0:T(2,128)S(1)}, f32[2,512]{1,0:T(2,128)}, u32[]{:S(2)}) copy-start(f32[2,512]{1,0:T(2,128)} %param.22) | copy-start | bytes 12292
  11.5 12.9 %copy-start.10 = (u32[32]{0:T(128)S(1)}, u32[32]{0:T(128)}, u32[]{:S(2)}) copy-start(u32[32]{0:T(128)} %constant.34) | copy-start | bytes 388
  11.5 40.2 %copy-start = (f32[2,4,8,64,64]{4,3,2,1,0:T(8,128)S(1)}, f32[2,4,8,64,64]{4,3,2,1,0:T(8,128)}, u32[]{:S(2)}) copy-start(f32[2,4,8,64,64]{4,3,2,1,0:T(8,128)} %param.13) | copy-start | bytes 3145732
  14.9 0.7 copy-start.6
  15.6 102.8 %all-reduce.7.cloned.1.call-start = ((), (), s32[]{:S(2)}) async-start(), calls=%async_computation.1 | async-start | bytes 393216
  62.7 4.3 %collective-permute-start = (f32[16,1024]{1,0:T(8,128)S(1)}, f32[16,1024]{1,0:T(8,128)S(1)}, u32[]{:S(2)}, u32[]{:S(2)}) collective-permute-start(f32[16,1024]{1,0:T(8,128)S(1)} %fusion.14), channel_id=1, source_target_pairs={{0,4},{4,0},{8,12},{12,8},{1,5},{5,1},{9,13},{13,9},{2,6},{6,2},{1... | collective-permute-start | bytes 196616 | tf_op jit(solution)/shard_map/ppermute | solution.py:57
  67.0 5.4 %collective-permute-start.1 = (f32[16,1024]{1,0:T(8,128)S(1)}, f32[16,1024]{1,0:T(8,128)S(1)}, u32[]{:S(2)}, u32[]{:S(2)}) collective-permute-start(f32[16,1024]{1,0:T(8,128)S(1)} %add.157), channel_id=1, source_target_pairs={{0,8},{4,12},{8,0},{12,4},{1,9},{5,13},{9,1},{13,5},{2,10},{6,14},... | collective-permute-start | bytes 196616 | tf_op jit(solution)/shard_map/ppermute | solution.py:57
  78.4 3.1 %copy-start.3 = (bf16[2,1024,512]{2,1,0:T(8,128)(2,1)S(1)}, bf16[2,1024,512]{2,1,0:T(8,128)(2,1)}, u32[]{:S(2)}) copy-start(bf16[2,1024,512]{2,1,0:T(8,128)(2,1)} %param.17) | copy-start | bytes 6291460
  78.4 4.8 %copy-start.5 = (bf16[2,1024,512]{2,1,0:T(8,128)(2,1)S(1)}, bf16[2,1024,512]{2,1,0:T(8,128)(2,1)}, u32[]{:S(2)}) copy-start(bf16[2,1024,512]{2,1,0:T(8,128)(2,1)} %param.19) | copy-start | bytes 6291460
  85.0 0.7 copy-start.7
  130.6 4.3 %collective-permute-start.2 = (f32[16,1024]{1,0:T(8,128)S(1)}, f32[16,1024]{1,0:T(8,128)S(1)}, u32[]{:S(2)}, u32[]{:S(2)}) collective-permute-start(f32[16,1024]{1,0:T(8,128)S(1)} %fusion), channel_id=1, source_target_pairs={{0,4},{4,0},{8,12},{12,8},{1,5},{5,1},{9,13},{13,9},{2,6},{6,2},{1... | collective-permute-start | bytes 196616 | tf_op jit(solution)/shard_map/ppermute | solution.py:57
  135.0 5.4 %collective-permute-start.3 = (f32[16,1024]{1,0:T(8,128)S(1)}, f32[16,1024]{1,0:T(8,128)S(1)}, u32[]{:S(2)}, u32[]{:S(2)}) collective-permute-start(f32[16,1024]{1,0:T(8,128)S(1)} %add.170), channel_id=1, source_target_pairs={{0,8},{4,12},{8,0},{12,4},{1,9},{5,13},{9,1},{13,5},{2,10},{6,14},... | collective-permute-start | bytes 196616 | tf_op jit(solution)/shard_map/ppermute | solution.py:57
Sparse Core Ops, SparseCore 0:
  15.7 34.7 all-reduce.4
  85.8 32.5 all-reduce.6
